TPU v7x, 32 devices: a whole 2x2x4 slice. The times are simulated.
32 devices in a mesh: sp: 8 (over z, x), dp: 4 (over y, core).
Axes of the slice: x: 2, y: 2, z: 4, core: 2. Of those that a mesh axis runs over, the one named last changes fastest.
Arguments:
- tokens: bfloat16 [4, 3072, 2048], P('dp', 'sp'), may hold values from -6 to 6
- q_weight: bfloat16 [2048, 1024], P(('sp', 'dp')), may hold values from -0.13258252 to 0.13258252
- k_weight: bfloat16 [2048, 256], P(('sp', 'dp')), may hold values from -0.13258252 to 0.13258252
- v_weight: bfloat16 [2048, 256], P(('sp', 'dp')), may hold values from -0.125 to 0.125
- out_weight: bfloat16 [1024, 2048], P(None, ('sp', 'dp')), may hold values from -6 to 6
- q_gain: float32 [64], replicated, may hold values from 0.5 to 8
- k_gain: float32 [64], replicated, may hold values from 0.5 to 8
Outputs:
- mixed: bfloat16 [4, 3072, 2048], P('dp', 'sp')
All inputs are finite; a program needn't handle non-finite values.
Results may differ from a plain program's by a relative error of at most 0.0055.
The roundings to bfloat16 on the way count: a program that leaves them out, or rounds other values in their place, can miss the bound.
Values may be sent and summed in bfloat16 or wider, within the bound.
A program may use at most 128 MiB of HBM per device.

v0:
```python
import math
import jax
import jax.numpy as jnp
from jax import lax
from jax.sharding import PartitionSpec as P

GRID_W = 64
epsilon = 1e-06
rope_base = 10000.0


def normalize(tensor, gain_vec):
    mean_sq = jnp.mean(tensor * tensor, axis=-1, keepdims=True)
    return tensor * lax.rsqrt(mean_sq + epsilon) * gain_vec


def rotate(tensor, offset):
    row_count = tensor.shape[0]
    head_width = tensor.shape[2]
    quarter = head_width // 4
    half_width = head_width // 2
    positions = jnp.arange(row_count, dtype=jnp.int32) + offset
    frequency = rope_base ** (-jnp.arange(quarter, dtype=jnp.float32) / quarter)

    def rotate_pair(segment, coords):
        angles = coords.astype(jnp.float32)[:, None] * frequency[None, :]
        cosine = jnp.cos(angles)[:, None, :]
        sine_val = jnp.sin(angles)[:, None, :]
        low_half = segment[..., :quarter]
        high_half = segment[..., quarter:]
        return jnp.concatenate(
            [low_half * cosine - high_half * sine_val, high_half * cosine + low_half * sine_val],
            axis=-1,
        )

    return jnp.concatenate(
        [
            rotate_pair(tensor[..., :half_width], positions // GRID_W),
            rotate_pair(tensor[..., half_width:], positions % GRID_W),
        ],
        axis=-1,
    )


def attend(query_rows, key_rows, value_rows):
    row_count, head_width = query_rows.shape
    block_rows = math.gcd(row_count, 512)
    score_scale = head_width ** (-0.5)

    def attend_block(segment):
        scores = (
            lax.dot_general(
                segment, key_rows, (((1,), (1,)), ((), ())), preferred_element_type=jnp.float32
            )
            * score_scale
        )
        row_max = jnp.max(scores, axis=-1, keepdims=True)
        weights = jnp.exp(scores - row_max)
        shares = (weights / jnp.sum(weights, axis=-1, keepdims=True)).astype(jnp.bfloat16)
        return jnp.dot(shares, value_rows, preferred_element_type=jnp.float32).astype(jnp.bfloat16)

    blocks = query_rows.reshape(row_count // block_rows, block_rows, head_width)
    return lax.map(attend_block, blocks).reshape(row_count, head_width)


def per_device(tokens, q_weight, k_weight, v_weight, out_weight, q_gain, k_gain):
    rows_in = tokens[0]
    tok_count = rows_in.shape[0]
    head_width = q_gain.shape[0]
    q_width = out_weight.shape[0]
    kv_width = k_weight.shape[1]
    q_heads = q_width // head_width
    kv_heads = kv_width // head_width
    group_size = q_heads // kv_heads
    sp_count = lax.axis_size("sp")
    offset = lax.axis_index("sp") * tok_count
    weight_rows = (
        lax.all_gather(q_weight, ("sp", "dp"), axis=0, tiled=True),
        lax.all_gather(k_weight, ("sp", "dp"), axis=0, tiled=True),
        lax.all_gather(v_weight, ("sp", "dp"), axis=0, tiled=True),
    )
    query_raw, key_raw, value_raw = tuple(
        (
            jnp.dot(rows_in, rows_part, preferred_element_type=jnp.float32)
            for rows_part in weight_rows
        )
    )
    queries = rotate(
        normalize(query_raw.reshape(tok_count, q_heads, head_width), q_gain), offset
    ).astype(jnp.bfloat16)
    keys_rot = rotate(
        normalize(key_raw.reshape(tok_count, kv_heads, head_width), k_gain), offset
    ).astype(jnp.bfloat16)
    values_dev = value_raw.astype(jnp.bfloat16)
    keys_wide = jnp.broadcast_to(
        keys_rot[:, :, None, :], (tok_count, kv_heads, group_size, head_width)
    ).reshape(tok_count, q_width)
    values_wide = jnp.broadcast_to(
        values_dev.reshape(tok_count, kv_heads, 1, head_width),
        (tok_count, kv_heads, group_size, head_width),
    ).reshape(tok_count, q_width)
    q_local, k_local, v_local = (
        lax.all_to_all(
            queries.reshape(tok_count, q_width), "sp", split_axis=1, concat_axis=0, tiled=True
        ),
        lax.all_to_all(keys_wide, "sp", split_axis=1, concat_axis=0, tiled=True),
        lax.all_to_all(values_wide, "sp", split_axis=1, concat_axis=0, tiled=True),
    )
    local_heads = q_width // sp_count // head_width
    outputs = []
    for head_index in range(local_heads):
        low_col = head_index * head_width
        outputs.append(
            attend(
                q_local[:, low_col : low_col + head_width],
                k_local[:, low_col : low_col + head_width],
                v_local[:, low_col : low_col + head_width],
            )
        )
    head_results = jnp.concatenate(outputs, axis=1)
    attended = lax.all_to_all(head_results, "sp", split_axis=0, concat_axis=1, tiled=True)
    result = jnp.dot(
        attended,
        lax.all_gather(out_weight, ("sp", "dp"), axis=1, tiled=True),
        preferred_element_type=jnp.float32,
    ).astype(jnp.bfloat16)
    return result[None]


def solution(mesh):
    return jax.shard_map(
        per_device,
        mesh=mesh,
        in_specs=(
            P("dp", "sp", None),
            P(("sp", "dp"), None),
            P(("sp", "dp"), None),
            P(("sp", "dp"), None),
            P(None, ("sp", "dp")),
            P(),
            P(),
        ),
        out_specs=P("dp", "sp", None),
        check_vma=False,
    )
```

profile of v0, /device:TPU:0, one launch (start us, length us, event | category | flops | bytes accessed | tf_op | source)
XLA Modules:
  0.0 334.7 jit_solution(1105141185171821577)
XLA Ops:
  9.0 57.6 %all-gather.7.cloned.1.call-done = bf16[2048,256]{1,0:T(8,128)(2,1)} async-done(((bf16[64,256]{1,0:T(8,128)(2,1)}), bf16[2048,256]{1,0:T(8,128)(2,1)}) %all-gather.7.cloned.1.call-update) | async-done | bytes 1048592 | tf_op jit(solution)/shard_map/all_gather | solution.py:79
  66.6 1.5 copy.28
  70.1 4.3 %all-to-all-start.1 = ((bf16[384,8,128]{0,2,1:T(8,128)(2,1)}), bf16[384,8,128]{0,2,1:T(8,128)(2,1)S(1)}, u32[]{:S(2)}, u32[]{:S(2)}) async-start(bf16[384,8,128]{0,2,1:T(8,128)(2,1)} %bitcast.14), calls=%async_computation.1 | async-start | bytes 1572864 | tf_op jit(solution)/shard_map/all_to_all | solution.py:106
  74.4 51.6 %all-gather.9.cloned.1.call-done = bf16[2048,256]{1,0:T(8,128)(2,1)} async-done(((bf16[64,256]{1,0:T(8,128)(2,1)}), bf16[2048,256]{1,0:T(8,128)(2,1)}) %all-gather.9.cloned.1.call-update) | async-done | bytes 1048592 | tf_op jit(solution)/shard_map/all_gather | solution.py:80
  126.0 2.0 fusion.27
  129.0 4.3 %all-to-all-start.2 = ((bf16[384,8,128]{0,2,1:T(8,128)(2,1)}), bf16[384,8,128]{0,2,1:T(8,128)(2,1)S(1)}, u32[]{:S(2)}, u32[]{:S(2)}) async-start(bf16[384,8,128]{0,2,1:T(8,128)(2,1)} %bitcast.90), calls=%async_computation.2 | async-start | bytes 1572864 | tf_op jit(solution)/shard_map/all_to_all | solution.py:107
  133.9 1.2 copy.29
  135.1 21.5 %all-to-all-done.2 = bf16[384,8,128]{0,2,1:T(8,128)(2,1)S(1)} async-done(((bf16[384,8,128]{0,2,1:T(8,128)(2,1)}), bf16[384,8,128]{0,2,1:T(8,128)(2,1)S(1)}, u32[]{:S(2)}, u32[]{:S(2)}) %all-to-all-start.2) | async-done | bytes 786464 | tf_op jit(solution)/shard_map/all_to_all | solution.py:107
  156.6 1.2 copy.30
  157.8 35.9 %all-gather.5.cloned.1.call-done = bf16[2048,1024]{1,0:T(8,128)(2,1)} async-done(((bf16[64,1024]{1,0:T(8,128)(2,1)}), bf16[2048,1024]{1,0:T(8,128)(2,1)}) %all-gather.5.cloned.1.call-update) | async-done | bytes 4194320 | tf_op jit(solution)/shard_map/all_gather | solution.py:78
  193.8 6.5 %copy.26 = bf16[1024,2048]{1,0:T(8,128)(2,1)} copy(bf16[1024,2048]{0,1:T(8,128)(2,1)} %bitcast.85) | data formatting | bytes 8388608 | tf_op jit(solution)/shard_map/dot_general | solution.py:84
  200.3 4.6 %multiply_reduce_fusion.2 = (f32[384,16]{0,1:T(8,128)S(1)}, f32[384,16,64]{0,2,1:T(8,128)S(1)}) fusion(bf16[16,64,2048]{2,1,0:T(8,128)(2,1)} %bitcast.86, bf16[1,384,2048]{2,1,0:T(8,128)(2,1)S(1)} %copy-done), kind=kOutput, calls=%fused_computation.35 | convolution fusion | flops 1611393024 | bytes 7364608 | tf_op jit(solution)/shard_map/dot_general | solution.py:84
  205.6 1.2 copy.27
  206.7 4.4 %all-to-all-start = ((bf16[384,8,128]{2,0,1:T(8,128)(2,1)}), bf16[384,8,128]{2,0,1:T(8,128)(2,1)}, u32[]{:S(2)}, u32[]{:S(2)}) async-start(bf16[384,8,128]{2,0,1:T(8,128)(2,1)} %copy.27), calls=%async_computation | async-start | bytes 1572864 | tf_op jit(solution)/shard_map/all_to_all | solution.py:103
  211.2 1.7 fusion.36
  212.9 2.8 fusion.35
  215.7 20.6 %all-to-all-done = bf16[384,8,128]{2,0,1:T(8,128)(2,1)} async-done(((bf16[384,8,128]{2,0,1:T(8,128)(2,1)}), bf16[384,8,128]{2,0,1:T(8,128)(2,1)}, u32[]{:S(2)}, u32[]{:S(2)}) %all-to-all-start) | async-done | bytes 786464 | tf_op jit(solution)/shard_map/all_to_all | solution.py:103
  236.3 2.9 fusion.37
  239.2 28.8 %while.20 = (s32[]{:T(128)}, bf16[6,512,64]{1,2,0:T(8,128)(2,1)S(1)}, bf16[6,512,64]{2,1,0:T(8,128)(2,1)}, bf16[3072,64]{1,0:T(8,128)(2,1)S(1)}, bf16[3072,64]{1,0:T(8,128)(2,1)}, /*index=5*/s32[]{:T(128)}) while((s32[]{:T(128)}, bf16[6,512,64]{1,2,0:T(8,128)(2,1)S(1)}, bf16[6,512,64]{2,1,0:T(8,128)(2,1)}, bf16[3072,64]{1,0:T(8,128)(2,1)S(1)}, ...), condition=%wide.region_5.6_spmd, body=%wide.region_2.5_spmd.sunk | while | flops 416840704 | bytes 21834340 | solution.py:63
  239.3 2.0 multiply_reduce_fusion.6
  241.2 1.2 fusion.57
  242.4 1.6 fusion.58
  244.0 2.0 multiply_reduce_fusion.6
  247.2 1.6 fusion.58
  248.9 2.0 multiply_reduce_fusion.6
  252.0 1.6 fusion.58
  253.7 2.0 multiply_reduce_fusion.6
  256.8 1.6 fusion.58
  258.5 2.0 multiply_reduce_fusion.6
  261.7 1.6 fusion.58
  263.3 2.0 multiply_reduce_fusion.6
  266.4 1.6 fusion.58
  268.6 28.7 %while.21 = (s32[]{:T(128)}, bf16[6,512,64]{1,2,0:T(8,128)(2,1)S(1)}, bf16[6,512,64]{2,1,0:T(8,128)(2,1)}, bf16[3072,64]{1,0:T(8,128)(2,1)S(1)}, bf16[3072,64]{1,0:T(8,128)(2,1)}, /*index=5*/s32[]{:T(128)}) while((s32[]{:T(128)}, bf16[6,512,64]{1,2,0:T(8,128)(2,1)S(1)}, bf16[6,512,64]{2,1,0:T(8,128)(2,1)}, bf16[3072,64]{1,0:T(8,128)(2,1)S(1)}, ...), condition=%wide.region_9.10_spmd, body=%wide.region_6.9_spmd.sunk | while | flops 416840704 | bytes 21834340 | solution.py:63
  268.6 2.0 multiply_reduce_fusion.7
  271.8 1.6 fusion.62
  273.4 2.0 multiply_reduce_fusion.7
  276.5 1.6 fusion.62
  278.2 2.0 multiply_reduce_fusion.7
  281.3 1.6 fusion.62
  283.0 2.0 multiply_reduce_fusion.7
  286.1 1.6 fusion.62
  287.8 2.0 multiply_reduce_fusion.7
  290.9 1.6 fusion.62
  292.6 2.0 multiply_reduce_fusion.7
  295.7 1.6 fusion.62
  298.9 3.7 %all-to-all-start.3 = ((bf16[8,384,128]{1,2,0:T(8,128)(2,1)}), bf16[8,384,128]{1,2,0:T(8,128)(2,1)S(1)}, u32[]{:S(2)}, u32[]{:S(2)}) async-start(bf16[8,384,128]{1,2,0:T(8,128)(2,1)} %copy.33), calls=%async_computation.3 | async-start | bytes 1572864 | tf_op jit(solution)/shard_map/all_to_all | solution.py:121
  302.6 20.4 %all-to-all-done.3 = bf16[8,384,128]{1,2,0:T(8,128)(2,1)S(1)} async-done(((bf16[8,384,128]{1,2,0:T(8,128)(2,1)}), bf16[8,384,128]{1,2,0:T(8,128)(2,1)S(1)}, u32[]{:S(2)}, u32[]{:S(2)}) %all-to-all-start.3) | async-done | bytes 786464 | tf_op jit(solution)/shard_map/all_to_all | solution.py:121
  323.0 5.2 %fusion.20 = bf16[1,384,2048]{2,1,0:T(8,128)(2,1)} fusion(bf16[384,1024]{0,1:T(8,128)(2,1)S(1)} %bitcast.95, bf16[1024,2048]{0,1:T(8,128)(2,1)} %all-gather.11.cloned.1.call-done), kind=kOutput, calls=%fused_computation.27 | convolution fusion | flops 1611399168 | bytes 6553600 | tf_op jit(solution)/shard_map/dot_general | solution.py:122
  (73 shorter events, 21.5 us)
Async XLA Ops:
  6.5 61.6 %copy-start = (bf16[1,384,2048]{2,1,0:T(8,128)(2,1)S(1)}, bf16[1,384,2048]{2,1,0:T(8,128)(2,1)}, u32[]{:S(2)}) copy-start(bf16[1,384,2048]{2,1,0:T(8,128)(2,1)} %param.11) | copy-start | bytes 4718596
  6.5 62.4 %copy-start.3 = (f32[64]{0:T(128)S(1)}, f32[64]{0:T(128)}, u32[]{:S(2)}) copy-start(f32[64]{0:T(128)} %param.17) | copy-start | bytes 772
  6.5 60.1 %all-gather.7.cloned.1.call-start = ((), (), s32[]{:S(2)}) async-start(), calls=%async_computation.5 | async-start | bytes 1081344 | tf_op jit(solution)/shard_map/all_gather | solution.py:79
  7.3 118.8 %all-gather.9.cloned.1.call-start = ((), (), s32[]{:S(2)}) async-start(), calls=%async_computation.6 | async-start | bytes 1081344 | tf_op jit(solution)/shard_map/all_gather | solution.py:80
  8.0 185.8 %all-gather.5.cloned.1.call-start = ((), (), s32[]{:S(2)}) async-start(), calls=%async_computation.4 | async-start | bytes 4325376 | tf_op jit(solution)/shard_map/all_gather | solution.py:78
  70.1 57.9 %all-to-all-start.1 = ((bf16[384,8,128]{0,2,1:T(8,128)(2,1)}), bf16[384,8,128]{0,2,1:T(8,128)(2,1)S(1)}, u32[]{:S(2)}, u32[]{:S(2)}) async-start(bf16[384,8,128]{0,2,1:T(8,128)(2,1)} %bitcast.14), calls=%async_computation.1 | async-start | bytes 1572864 | tf_op jit(solution)/shard_map/all_to_all | solution.py:106
  129.0 27.6 %all-to-all-start.2 = ((bf16[384,8,128]{0,2,1:T(8,128)(2,1)}), bf16[384,8,128]{0,2,1:T(8,128)(2,1)S(1)}, u32[]{:S(2)}, u32[]{:S(2)}) async-start(bf16[384,8,128]{0,2,1:T(8,128)(2,1)} %bitcast.90), calls=%async_computation.2 | async-start | bytes 1572864 | tf_op jit(solution)/shard_map/all_to_all | solution.py:107
  133.3 169.3 %all-gather.11.cloned.1.call-start = ((), (), s32[]{:S(2)}) async-start(), calls=%async_computation.7 | async-start | bytes 4325376 | tf_op jit(solution)/shard_map/all_gather | solution.py:124
  200.3 4.6 %copy-start.4 = (f32[64]{0:T(128)S(1)}, f32[64]{0:T(128)}, u32[]{:S(2)}) copy-start(f32[64]{0:T(128)} %param.16) | copy-start | bytes 772
  206.7 29.6 %all-to-all-start = ((bf16[384,8,128]{2,0,1:T(8,128)(2,1)}), bf16[384,8,128]{2,0,1:T(8,128)(2,1)}, u32[]{:S(2)}, u32[]{:S(2)}) async-start(bf16[384,8,128]{2,0,1:T(8,128)(2,1)} %copy.27), calls=%async_computation | async-start | bytes 1572864 | tf_op jit(solution)/shard_map/all_to_all | solution.py:103
  241.2 1.2 copy-start.2
  246.1 1.2 copy-start.2
  250.9 1.2 copy-start.2
  255.7 1.2 copy-start.2
  260.4 1.2 copy-start.2
  265.3 1.2 copy-start.2
  270.6 1.2 copy-start.1
  275.4 1.2 copy-start.1
  280.2 1.2 copy-start.1
  285.0 1.2 copy-start.1
  289.8 1.2 copy-start.1
  294.5 1.2 copy-start.1
  298.9 24.1 %all-to-all-start.3 = ((bf16[8,384,128]{1,2,0:T(8,128)(2,1)}), bf16[8,384,128]{1,2,0:T(8,128)(2,1)S(1)}, u32[]{:S(2)}, u32[]{:S(2)}) async-start(bf16[8,384,128]{1,2,0:T(8,128)(2,1)} %copy.33), calls=%async_computation.3 | async-start | bytes 1572864 | tf_op jit(solution)/shard_map/all_to_all | solution.py:121
Sparse Core Ops, SparseCore 0:
  10.2 56.3 all-gather.6
  69.5 56.4 all-gather.8
  128.9 64.7 all-gather.4
  196.5 66.2 all-gather.10
where the time goes:
time: 336 us; the launch traced here: 335 us
  waiting for transfers between devices  210 us (62%)
  matrix products  55.7 us (17%)
  local copies, waits for them, and re-layouts  23 us (7%)
  starting transfers between devices  16.8 us (5%)
  other arithmetic  15.1 us (4%)
  between operations  13.3 us (4%)
    all_gather x1, waiting for transfers between devices, per_device(): lax.all_gather(k_weight, ('sp', 'dp'), axis=0, tiled=True)  57.6 us
    all_gather x1, waiting for transfers between devices, per_device(): lax.all_gather(v_weight, ('sp', 'dp'), axis=0, tiled=True)  51.6 us
    all_gather x1, waiting for transfers between devices, per_device(): lax.all_gather(q_weight, ('sp', 'dp'), axis=0, tiled=True)  35.9 us
    dot_general x12, matrix products, attend_block(): lax.dot_general(segment, key_rows, (((1,), (1,)), ((), ())), preferred_el...  23.7 us
    all_to_all x1, waiting for transfers between devices, per_device(): lax.all_to_all(values_wide, 'sp', split_axis=1, concat_axis=0, tiled=True)  21.5 us
    all_to_all x1, waiting for transfers between devices, per_device(): lax.all_to_all(queries.reshape(tok_count, q_width), 'sp', split_axis=1, c...  20.6 us
    all_to_all x1, waiting for transfers between devices, per_device(): lax.all_to_all(head_results, 'sp', split_axis=0, concat_axis=1, tiled=True)  20.4 us
    dot_general x12, matrix products, attend_block(): jnp.dot(shares, value_rows, preferred_element_type=jnp.float32)  19.5 us
  transfers between devices with their start and end apart: 8, of which 6 were waited for; matrix products, arithmetic and copies ran while one was open for 26% of the time, Pallas kernels for 0%

commit v1 on v0

--- a/solution.py
+++ b/solution.py
@@ -7,6 +7,13 @@
 GRID_W = 64
 epsilon = 1e-06
 rope_base = 10000.0
+
+
+def stacked_exchange(value, axis, split, join):
+    peers = lax.axis_size(axis)
+    blocks = jnp.stack(jnp.split(value, peers, axis=split), axis=0)
+    blocks = lax.all_to_all(blocks, axis, split_axis=0, concat_axis=0)
+    return jnp.concatenate(blocks, axis=join)
 
 
 def normalize(tensor, gain_vec):
@@ -100,9 +107,7 @@
         (tok_count, kv_heads, group_size, head_width),
     ).reshape(tok_count, q_width)
     q_local, k_local, v_local = (
-        lax.all_to_all(
-            queries.reshape(tok_count, q_width), "sp", split_axis=1, concat_axis=0, tiled=True
-        ),
+        stacked_exchange(queries.reshape(tok_count, q_width), "sp", 1, 0),
         lax.all_to_all(keys_wide, "sp", split_axis=1, concat_axis=0, tiled=True),
         lax.all_to_all(values_wide, "sp", split_axis=1, concat_axis=0, tiled=True),
     )

time: 336 us -> 342 us (1.018)
  local copies, waits for them, and re-layouts: 23 us -> 28.1 us
    unnamed x6 -> x21, local copies, waits for them, and re-layouts: 0.01 us -> 5.56 us
  transfers between devices with their start and end apart: 8 -> 8, of which waited for: 6 -> 6; matrix products, arithmetic and copies ran while one was open for 26% -> 27% of each run, Pallas kernels for 0% -> 0%
where the time goes in v1:
time: 342 us; the launch traced here: 341 us
  waiting for transfers between devices  211 us (62%)
  matrix products  55.7 us (16%)
  local copies, waits for them, and re-layouts  28.1 us (8%)
  starting transfers between devices  16.7 us (5%)
  other arithmetic  15.1 us (4%)
  between operations  13.4 us (4%)
    all_gather x1, waiting for transfers between devices, per_device(): lax.all_gather(k_weight, ('sp', 'dp'), axis=0, tiled=True)  57.6 us
    all_gather x1, waiting for transfers between devices, per_device(): lax.all_gather(v_weight, ('sp', 'dp'), axis=0, tiled=True)  51.6 us
    all_gather x1, waiting for transfers between devices, per_device(): lax.all_gather(q_weight, ('sp', 'dp'), axis=0, tiled=True)  35.9 us
    dot_general x12, matrix products, attend_block(): lax.dot_general(segment, key_rows, (((1,), (1,)), ((), ())), preferred_el...  23.7 us
    all_to_all x1, waiting for transfers between devices, stacked_exchange(): blocks = lax.all_to_all(blocks, axis, split_axis=0, concat_axis=0)  21.7 us
    all_to_all x1, waiting for transfers between devices, per_device(): lax.all_to_all(values_wide, 'sp', split_axis=1, concat_axis=0, tiled=True)  21.6 us
    all_to_all x1, waiting for transfers between devices, per_device(): lax.all_to_all(head_results, 'sp', split_axis=0, concat_axis=1, tiled=True)  20.4 us
    dot_general x12, matrix products, attend_block(): jnp.dot(shares, value_rows, preferred_element_type=jnp.float32)  19.5 us
  transfers between devices with their start and end apart: 8, of which 6 were waited for; matrix products, arithmetic and copies ran while one was open for 27% of the time, Pallas kernels for 0%

profile of v1, /device:TPU:0, one launch (start us, length us, event | category | flops | bytes accessed | tf_op | source)
XLA Modules:
  0.0 340.9 jit_solution(4367314462959582382)
XLA Ops:
  9.0 57.6 %all-gather.7.cloned.1.call-done = bf16[2048,256]{1,0:T(8,128)(2,1)} async-done(((bf16[64,256]{1,0:T(8,128)(2,1)}), bf16[2048,256]{1,0:T(8,128)(2,1)}) %all-gather.7.cloned.1.call-update) | async-done | bytes 1048592 | tf_op jit(solution)/shard_map/all_gather | solution.py:86
  66.6 1.5 copy.49
  70.1 4.3 %all-to-all-start.1 = ((bf16[384,8,128]{0,2,1:T(8,128)(2,1)}), bf16[384,8,128]{0,2,1:T(8,128)(2,1)S(1)}, u32[]{:S(2)}, u32[]{:S(2)}) async-start(bf16[384,8,128]{0,2,1:T(8,128)(2,1)} %bitcast.21), calls=%async_computation.1 | async-start | bytes 1572864 | tf_op jit(solution)/shard_map/all_to_all | solution.py:111
  74.4 51.6 %all-gather.9.cloned.1.call-done = bf16[2048,256]{1,0:T(8,128)(2,1)} async-done(((bf16[64,256]{1,0:T(8,128)(2,1)}), bf16[2048,256]{1,0:T(8,128)(2,1)}) %all-gather.9.cloned.1.call-update) | async-done | bytes 1048592 | tf_op jit(solution)/shard_map/all_gather | solution.py:87
  126.0 2.0 fusion.27
  129.0 4.3 %all-to-all-start.2 = ((bf16[384,8,128]{0,2,1:T(8,128)(2,1)}), bf16[384,8,128]{0,2,1:T(8,128)(2,1)S(1)}, u32[]{:S(2)}, u32[]{:S(2)}) async-start(bf16[384,8,128]{0,2,1:T(8,128)(2,1)} %bitcast.104), calls=%async_computation.2 | async-start | bytes 1572864 | tf_op jit(solution)/shard_map/all_to_all | solution.py:112
  133.9 1.2 copy.50
  135.1 21.6 %all-to-all-done.2 = bf16[384,8,128]{0,2,1:T(8,128)(2,1)S(1)} async-done(((bf16[384,8,128]{0,2,1:T(8,128)(2,1)}), bf16[384,8,128]{0,2,1:T(8,128)(2,1)S(1)}, u32[]{:S(2)}, u32[]{:S(2)}) %all-to-all-start.2) | async-done | bytes 786464 | tf_op jit(solution)/shard_map/all_to_all | solution.py:112
  156.6 1.2 copy.51
  157.8 35.9 %all-gather.5.cloned.1.call-done = bf16[2048,1024]{1,0:T(8,128)(2,1)} async-done(((bf16[64,1024]{1,0:T(8,128)(2,1)}), bf16[2048,1024]{1,0:T(8,128)(2,1)}) %all-gather.5.cloned.1.call-update) | async-done | bytes 4194320 | tf_op jit(solution)/shard_map/all_gather | solution.py:85
  193.8 6.5 %copy.40 = bf16[1024,2048]{1,0:T(8,128)(2,1)} copy(bf16[1024,2048]{0,1:T(8,128)(2,1)} %bitcast.99) | data formatting | bytes 8388608 | tf_op jit(solution)/shard_map/dot_general | solution.py:91
  200.3 4.6 %multiply_reduce_fusion.2 = (f32[384,16]{0,1:T(8,128)S(1)}, f32[384,16,64]{0,2,1:T(8,128)S(1)}) fusion(bf16[16,64,2048]{2,1,0:T(8,128)(2,1)} %bitcast.100, bf16[1,384,2048]{2,1,0:T(8,128)(2,1)S(1)} %copy-done), kind=kOutput, calls=%fused_computation.35 | convolution fusion | flops 1611393024 | bytes 7364608 | tf_op jit(solution)/shard_map/dot_general | solution.py:91
  211.9 4.4 %all-to-all-start = ((bf16[8,384,128]{2,1,0:T(8,128)(2,1)}), bf16[8,384,128]{2,1,0:T(8,128)(2,1)}, u32[]{:S(2)}, u32[]{:S(2)}) async-start(bf16[8,384,128]{2,1,0:T(8,128)(2,1)} %bitcast_dynamic-update-slice_fusion), calls=%async_computation | async-start | bytes 1572864 | tf_op jit(solution)/shard_map/all_to_all | solution.py:15
  216.3 1.7 fusion.36
  218.0 2.8 fusion.35
  220.9 21.7 %all-to-all-done = bf16[8,384,128]{2,1,0:T(8,128)(2,1)} async-done(((bf16[8,384,128]{2,1,0:T(8,128)(2,1)}), bf16[8,384,128]{2,1,0:T(8,128)(2,1)}, u32[]{:S(2)}, u32[]{:S(2)}) %all-to-all-start) | async-done | bytes 786464 | tf_op jit(solution)/shard_map/all_to_all | solution.py:15
  242.6 2.9 fusion.37
  245.5 28.8 %while.20 = (s32[]{:T(128)}, bf16[6,512,64]{1,2,0:T(8,128)(2,1)S(1)}, bf16[6,512,64]{2,1,0:T(8,128)(2,1)}, bf16[3072,64]{1,0:T(8,128)(2,1)S(1)}, bf16[3072,64]{1,0:T(8,128)(2,1)}, /*index=5*/s32[]{:T(128)}) while((s32[]{:T(128)}, bf16[6,512,64]{1,2,0:T(8,128)(2,1)S(1)}, bf16[6,512,64]{2,1,0:T(8,128)(2,1)}, bf16[3072,64]{1,0:T(8,128)(2,1)S(1)}, ...), condition=%wide.region_5.6_spmd, body=%wide.region_2.5_spmd.sunk | while | flops 416840704 | bytes 21834340 | solution.py:70
  245.5 2.0 multiply_reduce_fusion.6
  248.7 1.6 fusion.59
  250.3 2.0 multiply_reduce_fusion.6
  253.5 1.6 fusion.59
  255.1 2.0 multiply_reduce_fusion.6
  258.3 1.6 fusion.59
  259.9 2.0 multiply_reduce_fusion.6
  263.1 1.6 fusion.59
  264.7 2.0 multiply_reduce_fusion.6
  267.9 1.6 fusion.59
  269.5 2.0 multiply_reduce_fusion.6
  272.7 1.6 fusion.59
  274.8 28.7 %while.21 = (s32[]{:T(128)}, bf16[6,512,64]{1,2,0:T(8,128)(2,1)S(1)}, bf16[6,512,64]{2,1,0:T(8,128)(2,1)}, bf16[3072,64]{1,0:T(8,128)(2,1)S(1)}, bf16[3072,64]{1,0:T(8,128)(2,1)}, /*index=5*/s32[]{:T(128)}) while((s32[]{:T(128)}, bf16[6,512,64]{1,2,0:T(8,128)(2,1)S(1)}, bf16[6,512,64]{2,1,0:T(8,128)(2,1)}, bf16[3072,64]{1,0:T(8,128)(2,1)S(1)}, ...), condition=%wide.region_9.10_spmd, body=%wide.region_6.9_spmd.sunk | while | flops 416840704 | bytes 21834340 | solution.py:70
  274.8 2.0 multiply_reduce_fusion.7
  278.0 1.6 fusion.63
  279.6 2.0 multiply_reduce_fusion.7
  281.6 1.2 fusion.62
  282.8 1.6 fusion.63
  284.4 2.0 multiply_reduce_fusion.7
  287.6 1.6 fusion.63
  289.2 2.0 multiply_reduce_fusion.7
  291.2 1.2 fusion.62
  292.4 1.6 fusion.63
  294.0 2.0 multiply_reduce_fusion.7
  297.2 1.6 fusion.63
  298.8 2.0 multiply_reduce_fusion.7
  301.9 1.6 fusion.63
  305.2 3.6 %all-to-all-start.3 = ((bf16[8,384,128]{1,2,0:T(8,128)(2,1)}), bf16[8,384,128]{1,2,0:T(8,128)(2,1)S(1)}, u32[]{:S(2)}, u32[]{:S(2)}) async-start(bf16[8,384,128]{1,2,0:T(8,128)(2,1)} %copy.54), calls=%async_computation.3 | async-start | bytes 1572864 | tf_op jit(solution)/shard_map/all_to_all | solution.py:126
  308.8 20.4 %all-to-all-done.3 = bf16[8,384,128]{1,2,0:T(8,128)(2,1)S(1)} async-done(((bf16[8,384,128]{1,2,0:T(8,128)(2,1)}), bf16[8,384,128]{1,2,0:T(8,128)(2,1)S(1)}, u32[]{:S(2)}, u32[]{:S(2)}) %all-to-all-start.3) | async-done | bytes 786464 | tf_op jit(solution)/shard_map/all_to_all | solution.py:126
  329.2 5.2 %fusion.20 = bf16[1,384,2048]{2,1,0:T(8,128)(2,1)} fusion(bf16[384,1024]{0,1:T(8,128)(2,1)S(1)} %bitcast.109, bf16[1024,2048]{0,1:T(8,128)(2,1)} %all-gather.11.cloned.1.call-done), kind=kOutput, calls=%fused_computation.27 | convolution fusion | flops 1611399168 | bytes 6553600 | tf_op jit(solution)/shard_map/dot_general | solution.py:127
  (89 shorter events, 26.6 us)
Async XLA Ops:
  6.5 61.6 %copy-start = (bf16[1,384,2048]{2,1,0:T(8,128)(2,1)S(1)}, bf16[1,384,2048]{2,1,0:T(8,128)(2,1)}, u32[]{:S(2)}) copy-start(bf16[1,384,2048]{2,1,0:T(8,128)(2,1)} %param.11) | copy-start | bytes 4718596
  6.5 62.4 %copy-start.3 = (f32[64]{0:T(128)S(1)}, f32[64]{0:T(128)}, u32[]{:S(2)}) copy-start(f32[64]{0:T(128)} %param.17) | copy-start | bytes 772
  6.5 60.1 %all-gather.7.cloned.1.call-start = ((), (), s32[]{:S(2)}) async-start(), calls=%async_computation.5 | async-start | bytes 1081344 | tf_op jit(solution)/shard_map/all_gather | solution.py:86
  7.3 118.8 %all-gather.9.cloned.1.call-start = ((), (), s32[]{:S(2)}) async-start(), calls=%async_computation.6 | async-start | bytes 1081344 | tf_op jit(solution)/shard_map/all_gather | solution.py:87
  8.0 185.8 %all-gather.5.cloned.1.call-start = ((), (), s32[]{:S(2)}) async-start(), calls=%async_computation.4 | async-start | bytes 4325376 | tf_op jit(solution)/shard_map/all_gather | solution.py:85
  70.1 57.9 %all-to-all-start.1 = ((bf16[384,8,128]{0,2,1:T(8,128)(2,1)}), bf16[384,8,128]{0,2,1:T(8,128)(2,1)S(1)}, u32[]{:S(2)}, u32[]{:S(2)}) async-start(bf16[384,8,128]{0,2,1:T(8,128)(2,1)} %bitcast.21), calls=%async_computation.1 | async-start | bytes 1572864 | tf_op jit(solution)/shard_map/all_to_all | solution.py:111
  129.0 27.6 %all-to-all-start.2 = ((bf16[384,8,128]{0,2,1:T(8,128)(2,1)}), bf16[384,8,128]{0,2,1:T(8,128)(2,1)S(1)}, u32[]{:S(2)}, u32[]{:S(2)}) async-start(bf16[384,8,128]{0,2,1:T(8,128)(2,1)} %bitcast.104), calls=%async_computation.2 | async-start | bytes 1572864 | tf_op jit(solution)/shard_map/all_to_all | solution.py:112
  133.3 175.4 %all-gather.11.cloned.1.call-start = ((), (), s32[]{:S(2)}) async-start(), calls=%async_computation.7 | async-start | bytes 4325376 | tf_op jit(solution)/shard_map/all_gather | solution.py:129
  200.2 4.6 %copy-start.4 = (f32[64]{0:T(128)S(1)}, f32[64]{0:T(128)}, u32[]{:S(2)}) copy-start(f32[64]{0:T(128)} %param.16) | copy-start | bytes 772
  211.9 30.7 %all-to-all-start = ((bf16[8,384,128]{2,1,0:T(8,128)(2,1)}), bf16[8,384,128]{2,1,0:T(8,128)(2,1)}, u32[]{:S(2)}, u32[]{:S(2)}) async-start(bf16[8,384,128]{2,1,0:T(8,128)(2,1)} %bitcast_dynamic-update-slice_fusion), calls=%async_computation | async-start | bytes 1572864 | tf_op jit(solution)/shard_map/all_to_all | solution.py:15
  247.5 1.2 copy-start.2
  252.3 1.2 copy-start.2
  257.1 1.2 copy-start.2
  261.9 1.2 copy-start.2
  266.7 1.2 copy-start.2
  271.5 1.2 copy-start.2
  276.8 1.2 copy-start.1
  281.6 1.2 copy-start.1
  286.4 1.2 copy-start.1
  291.2 1.2 copy-start.1
  296.0 1.2 copy-start.1
  300.8 1.2 copy-start.1
  305.2 24.0 %all-to-all-start.3 = ((bf16[8,384,128]{1,2,0:T(8,128)(2,1)}), bf16[8,384,128]{1,2,0:T(8,128)(2,1)S(1)}, u32[]{:S(2)}, u32[]{:S(2)}) async-start(bf16[8,384,128]{1,2,0:T(8,128)(2,1)} %copy.54), calls=%async_computation.3 | async-start | bytes 1572864 | tf_op jit(solution)/shard_map/all_to_all | solution.py:126
Sparse Core Ops, SparseCore 0:
  10.2 56.3 all-gather.6
  69.5 56.4 all-gather.8
  128.9 64.7 all-gather.4
  196.5 65.7 all-gather.10
